TPU v7x, 32 devices: a whole 2x2x4 slice. The times are simulated.
32 devices in a mesh: grp: 2 (over y), dp: 2 (over x), kv: 4 (over z), tp: 2 (over core).
Axes of the slice: x: 2, y: 2, z: 4, core: 2. Of those that a mesh axis runs over, the one named last changes fastest.
Arguments:
- inputs: bfloat16 [32, 4096], P(('grp', 'dp'), 'kv'), parts along dimension 0, may hold values from -6 to 6
- gain_in: float32 [4096], P('kv'), may hold values from 0.1 to 1.9
- w_gate: bfloat16 [4096, 2048], P('kv', 'tp'), may hold values from -0.09375 to 0.09375
- w_input: bfloat16 [4096, 2048], P('kv', 'tp'), may hold values from -0.09375 to 0.09375
- w_bproj: bfloat16 [4096, 1024], P('kv', 'tp'), may hold values from -0.09375 to 0.09375
- w_cproj: bfloat16 [4096, 1024], P('kv', 'tp'), may hold values from -0.09375 to 0.09375
- w_step: bfloat16 [4096, 32], P('kv', 'tp'), may hold values from -0.09375 to 0.09375
- conv_input: float32 [4, 2048], P(None, 'tp'), may hold values from -3 to 3
- conv_bproj: float32 [4, 1024], P(None, 'tp'), may hold values from -3 to 3
- conv_cproj: float32 [4, 1024], P(None, 'tp'), may hold values from -3 to 3
- tail_input: bfloat16 [32, 3, 2048], P(('grp', 'dp', 'kv'), None, 'tp'), parts along dimension 0, may hold values from -6 to 6
- tail_bproj: bfloat16 [32, 3, 1024], P(('grp', 'dp', 'kv'), None, 'tp'), parts along dimension 0, may hold values from -6 to 6
- tail_cproj: bfloat16 [32, 3, 1024], P(('grp', 'dp', 'kv'), None, 'tp'), parts along dimension 0, may hold values from -6 to 6
- step_bias: float32 [32], P('tp'), may hold values from -3 to 0
- decay_log: float32 [32], P('tp'), may hold values from -2 to 2
- block_input: bfloat16 [32, 128, 2048], P(('grp', 'dp', 'kv'), None, 'tp'), parts along dimension 0, may hold values from -6 to 6
- block_bproj: bfloat16 [32, 128, 1024], P(('grp', 'dp', 'kv'), None, 'tp'), parts along dimension 0, may hold values from -0.59765625 to 0.59765625
- block_step: float32 [32, 128, 32], P(('grp', 'dp', 'kv'), None, 'tp'), parts along dimension 0, may hold values from 0.005 to 0.2
- lengths: int32 [32], P(('grp', 'dp', 'kv')), parts along dimension 0, may hold values from 1 to 127, 512 in all
- state: float32 [32, 32, 64, 128], P(('grp', 'dp', 'kv'), 'tp'), parts along dimension 0, may hold values from -0.6 to 0.6
- gain_mix: float32 [2048], P('tp'), may hold values from 0.1 to 1.9
- w_out: bfloat16 [2048, 4096], P('tp', 'kv'), may hold values from -0.125 to 0.125
- gain_mlp: float32 [4096], P(('kv', 'tp')), may hold values from 0.1 to 1.9
- w_up: bfloat16 [4096, 16384], P(('kv', 'tp'), 'dp'), may hold values from -0.09375 to 0.09375
- w_down: bfloat16 [16384, 4096], P('dp', ('kv', 'tp')), may hold values from -0.046875 to 0.046875
Outputs:
- layer_out: bfloat16 [32, 4096], P(('grp', 'dp'), ('kv', 'tp')), parts along dimension 0
There are 2 independent parts, one for each index of `grp`. A program takes and returns all parts, laid end to end along the dimension named above; an argument that names none is the same for every part. Nothing has to cross between parts.
Inputs may be any that keep to these rules, and one draw needn't show every extreme that they name: `lengths`: the number of live positions before the new token in each sequence's current block; the largest equals 127 in every draw.
All inputs are finite; a program needn't handle non-finite values.
Results may differ from a plain program's by a relative error of at most 0.012.
Values may be sent and summed in bfloat16 or wider, within the bound.
A program may use at most 64 MiB of HBM per device.

v0:
```python
import jax
import jax.numpy as jnp
from jax import lax
from jax.sharding import PartitionSpec as P

D = 4096
HEAD_DIM = 64
D_STATE = 128
TAPS = 4
SSM_WIDTH = 2048


EPS = 1e-06


def convolve(history, weights, newest):
    summed = weights[TAPS - 1] * newest
    for offset in range(TAPS - 1):
        summed = summed + weights[offset] * history[:, offset].astype(jnp.float32)
    return jax.nn.silu(summed)


def per_device(
    inputs,
    gain_in,
    w_gate,
    w_input,
    w_bproj,
    w_cproj,
    w_step,
    conv_input,
    conv_bproj,
    conv_cproj,
    tail_input,
    tail_bproj,
    tail_cproj,
    step_bias,
    decay_log,
    block_input,
    block_bproj,
    block_step,
    lengths,
    state,
    gain_mix,
    w_out,
    gain_mlp,
    w_up,
    w_down,
):
    stream = inputs.astype(jnp.float32)
    squares = jnp.sum(stream * stream, axis=1)
    scaled = (stream * gain_in).astype(jnp.bfloat16)
    matrices = (w_gate, w_input, w_bproj, w_cproj, w_step)
    pieces = [jnp.dot(scaled, weight, preferred_element_type=jnp.float32) for weight in matrices]
    projected, totals = (
        lax.psum_scatter(jnp.concatenate(pieces, axis=1), "kv", scatter_dimension=0, tiled=True),
        lax.psum_scatter(squares, "kv", scatter_dimension=0, tiled=True),
    )
    inverse = lax.rsqrt(totals / D + EPS)[:, None]
    bounds = [0]
    for weight in matrices:
        bounds.append(bounds[-1] + weight.shape[1])
    gate_pre, value_pre, b_pre, c_pre, step_pre = [
        projected[:, bounds[member] : bounds[member + 1]] * inverse for member in range(5)
    ]
    seq_count = lengths.shape[0]
    head_count = step_bias.shape[0]
    group_count = w_bproj.shape[1] // D_STATE
    block_len = block_step.shape[1]
    per_group = head_count // group_count
    current = convolve(tail_input, conv_input, value_pre)
    b_now = convolve(tail_bproj, conv_bproj, b_pre)
    c_now = convolve(tail_cproj, conv_cproj, c_pre)
    step_size = jax.nn.softplus(step_pre + step_bias)
    decay_rate = -jnp.exp(decay_log)
    positions = lax.broadcasted_iota(jnp.int32, (1, block_len), 1)
    live_rows = (positions < lengths[:, None]).astype(jnp.float32)
    masked = block_step * live_rows[:, :, None]
    later_steps = jnp.sum(masked, axis=1, keepdims=True) - jnp.cumsum(masked, axis=1)
    decays = jnp.exp(decay_rate * (step_size[:, None, :] + later_steps)) * live_rows[:, :, None]
    c_query = c_now.astype(jnp.bfloat16).reshape(seq_count, group_count, D_STATE)
    keys = block_bproj.reshape(seq_count, block_len, group_count, D_STATE)
    scores = jnp.einsum("bsgn,bgn->bsg", keys, c_query, preferred_element_type=jnp.float32)
    scores = jnp.repeat(scores, per_group, axis=2)
    weights = (decays * scores * block_step).astype(jnp.bfloat16)
    values = block_input.reshape(seq_count, block_len, head_count, HEAD_DIM)
    inner_sum = jnp.einsum("bsh,bshp->bhp", weights, values, preferred_element_type=jnp.float32)
    c_full = c_now.reshape(seq_count, group_count, D_STATE)
    b_full = b_now.reshape(seq_count, group_count, D_STATE)
    own_score = jnp.repeat(jnp.sum(c_full * b_full, axis=2), per_group, axis=1)
    own_term = (step_size * own_score)[:, :, None] * current.reshape(
        seq_count, head_count, HEAD_DIM
    )
    carried = jnp.exp(decay_rate * (step_size + jnp.sum(masked, axis=1)))
    c_heads = jnp.repeat(c_full, per_group, axis=1)
    readout = jnp.einsum("bhpn,bhn->bhp", state, c_heads, precision=lax.Precision.HIGHEST)
    mixed = (inner_sum + own_term + carried[:, :, None] * readout).reshape(
        seq_count, -1
    ) * jax.nn.silu(gate_pre)
    local_sq = jnp.sum(mixed * mixed, axis=1)
    total_sq = lax.psum(local_sq, "tp")
    normed = (mixed * lax.rsqrt(total_sq / SSM_WIDTH + EPS)[:, None] * gain_mix).astype(
        jnp.bfloat16
    )
    products = jnp.dot(
        lax.all_gather(normed, "kv", axis=0, tiled=True), w_out, preferred_element_type=jnp.float32
    )
    mixed_in = lax.psum_scatter(products, "tp", scatter_dimension=1, tiled=True)
    column_count = mixed_in.shape[1]
    residual = lax.dynamic_slice_in_dim(
        stream, lax.axis_index("tp") * column_count, column_count, 1
    )
    hidden = (residual + mixed_in).astype(jnp.bfloat16)
    lifted = (hidden.astype(jnp.float32) * gain_mlp).astype(jnp.bfloat16)
    all_lifted, all_hidden = (
        lax.all_gather(lifted, "dp", axis=0, tiled=True),
        lax.all_gather(hidden, "dp", axis=0, tiled=True),
    )
    whole_rows = all_hidden.astype(jnp.float32)
    row_sq = jnp.sum(whole_rows * whole_rows, axis=1)
    partial_value = jnp.dot(all_lifted, w_up, preferred_element_type=jnp.float32)
    sq_sum = lax.psum(row_sq, ("kv", "tp"))
    shares = lax.psum_scatter(partial_value, ("kv", "tp"), scatter_dimension=1, tiled=True)
    unit_share = jnp.square(jax.nn.relu(shares * lax.rsqrt(sq_sum / D + EPS)[:, None])).astype(
        jnp.bfloat16
    )
    hidden_units = lax.all_gather(unit_share, ("kv", "tp"), axis=1, tiled=True)
    lowered = lax.psum_scatter(
        jnp.dot(hidden_units, w_down, preferred_element_type=jnp.float32),
        "dp",
        scatter_dimension=0,
        tiled=True,
    )
    return (hidden.astype(jnp.float32) + lowered).astype(jnp.bfloat16)


def solution(mesh):
    return jax.shard_map(
        per_device,
        mesh=mesh,
        in_specs=(
            P(("grp", "dp"), "kv"),
            P("kv"),
            P("kv", "tp"),
            P("kv", "tp"),
            P("kv", "tp"),
            P("kv", "tp"),
            P("kv", "tp"),
            P(None, "tp"),
            P(None, "tp"),
            P(None, "tp"),
            P(("grp", "dp", "kv"), None, "tp"),
            P(("grp", "dp", "kv"), None, "tp"),
            P(("grp", "dp", "kv"), None, "tp"),
            P("tp"),
            P("tp"),
            P(("grp", "dp", "kv"), None, "tp"),
            P(("grp", "dp", "kv"), None, "tp"),
            P(("grp", "dp", "kv"), None, "tp"),
            P(("grp", "dp", "kv")),
            P(("grp", "dp", "kv"), "tp", None, None),
            P("tp"),
            P("tp", "kv"),
            P(("kv", "tp")),
            P(("kv", "tp"), "dp"),
            P("dp", ("kv", "tp")),
        ),
        out_specs=P(("grp", "dp"), ("kv", "tp")),
        check_vma=False,
    )
```

profile of v0, /device:TPU:0, one launch (start us, length us, event | category | flops | bytes accessed | tf_op | source)
XLA Modules:
  0.0 172.6 jit_solution(11683976073686166705)
XLA Ops:
  6.5 1.6 copy-done
  12.3 14.1 %all-reduce.1 = f32[8]{0:T(128)} all-reduce(f32[8]{0:T(128)S(1)} %multiply_reduce_fusion.1), channel_id=3, replica_groups=mesh['grp'=2,'dp'=2,'kv'=4,'tp'=2] {'kv'}, use_global_device_ids=true, to_apply=%region_2.0.clone | all-reduce | flops 8 | bytes 64
  32.0 2.0 %copy.35 = bf16[2,128,1024]{1,2,0:T(8,128)(2,1)} copy(bf16[2,128,1024]{2,1,0:T(8,128)(2,1)} %param.40) | data formatting | bytes 1048576 | tf_op args[15]
  34.0 1.5 fusion.24
  37.4 1.9 %fusion.22 = (f32[2,16]{1,0:T(2,128)}, f32[2,128,16]{2,1,0:T(8,128)}) fusion(f32[2,128,16]{2,1,0:T(8,128)S(1)} %copy.32, f32[2,128]{1,0:T(2,128)} %compare_convert_fusion), kind=kLoop, calls=%fused_computation.64 | loop fusion | flops 8160 | bytes 33920 | tf_op jit(solution)/shard_map/reduce_sum | solution.py:79
  39.3 1.7 reduce_window_sum.11
  42.3 7.1 %all-reduce.4.cloned.1.call-done = f32[8,3088]{1,0:T(8,128)} async-done(((f32[8,3088]{1,0:T(8,128)}), f32[8,3088]{1,0:T(8,128)}) %all-reduce.4.cloned.1.call-update) | async-done | bytes 98832
  49.4 1.5 fusion.23
  54.9 1.3 reshape.89
  62.1 1.4 fusion.28
  64.2 1.7 %fusion.29 = f32[2,16,1,64]{3,2,1,0:T(1,128)S(1)} fusion(f32[2,16,128,1]{2,3,1,0:T(1,128)S(1)} %bitcast.82, f32[2,16,64,128]{3,2,1,0:T(8,128)S(1)} %copy-done.4), kind=kOutput, calls=%fused_computation.71 | convolution fusion | flops 3145728 | bytes 1073152 | tf_op jit(solution)/shard_map/bhpn,bhn->bhp/dot_general | solution.py:96
  67.1 2.5 %psum.14 = f32[2]{0:T(128)S(1)} all-reduce(f32[2]{0:T(128)S(1)} %get-tuple-element.7), channel_id=1, replica_groups=mesh['grp'=2,'dp'=2,'kv'=4,'tp'=2] {'tp'}, use_global_device_ids=true, to_apply=%region_7.8 | all-reduce | flops 2 | bytes 16 | tf_op jit(solution)/shard_map/psum | solution.py:101
  69.6 13.2 %all-gather = bf16[4,2,1024]{2,1,0:T(2,128)(2,1)S(1)} all-gather(bf16[1,2,1024]{2,1,0:T(2,128)(2,1)S(1)} %fusion.16), channel_id=1, replica_groups=mesh['grp'=2,'dp'=2,'kv'=4,'tp'=2] {'kv'}, dimensions={0}, use_global_device_ids=true | all-gather | bytes 20480 | tf_op jit(solution)/shard_map/all_gather | solution.py:106
  82.8 2.6 %fusion.30 = f32[8,1024]{1,0:T(8,128)} fusion(bf16[8,1024]{1,0:T(8,128)(2,1)S(1)} %reshape.103, bf16[1024,1024]{1,0:T(8,128)(2,1)} %param.46), kind=kOutput, calls=%fused_computation.72 | convolution fusion | flops 16777216 | bytes 2146304 | tf_op jit(solution)/shard_map/dot_general | solution.py:105
  85.5 7.6 %reduce-scatter.4.cloned.1.call-done = f32[8,512]{1,0:T(8,128)} async-done(((f32[8,1024]{1,0:T(8,128)}), f32[8,512]{1,0:T(8,128)}) %reduce-scatter.4.cloned.1.call-update) | async-done | bytes 16400 | tf_op jit(solution)/shard_map/reduce_scatter | solution.py:108
  93.9 4.3 %all_gather.13 = bf16[16,512]{1,0:T(8,128)(2,1)S(1)} all-gather(bf16[8,512]{1,0:T(8,128)(2,1)S(1)} %get-tuple-element.5), channel_id=1, replica_groups=mesh['grp'=2,'dp'=2,'kv'=4,'tp'=2] {'dp'}, dimensions={0}, use_global_device_ids=true | all-gather | bytes 24576 | tf_op jit(solution)/shard_map/all_gather | solution.py:116
  98.2 5.4 %fusion.31 = f32[16,8192]{1,0:T(8,128)} fusion(bf16[16,512]{1,0:T(8,128)(2,1)S(1)} %all_gather.13, bf16[512,8192]{1,0:T(8,128)(2,1)} %param.48), kind=kOutput, calls=%fused_computation.73 | convolution fusion | flops 134217728 | bytes 8929280 | tf_op jit(solution)/shard_map/dot_general | solution.py:121
  103.7 4.4 %all_gather.14 = bf16[16,512]{1,0:T(8,128)(2,1)S(1)} all-gather(bf16[8,512]{1,0:T(8,128)(2,1)S(1)} %get-tuple-element.6), channel_id=1, replica_groups=mesh['grp'=2,'dp'=2,'kv'=4,'tp'=2] {'dp'}, dimensions={0}, use_global_device_ids=true | all-gather | bytes 24576 | tf_op jit(solution)/shard_map/all_gather | solution.py:117
  108.1 14.8 %psum.15 = f32[16]{0:T(128)S(1)} all-reduce(f32[16]{0:T(128)S(1)} %multiply_reduce_fusion), channel_id=1, replica_groups=mesh['grp'=2,'dp'=2,'kv'=4,'tp'=2] {'kv','tp'}, use_global_device_ids=true, to_apply=%region_11.12 | all-reduce | flops 16 | bytes 128 | tf_op jit(solution)/shard_map/psum | solution.py:122
  123.0 13.2 %reduce-scatter.6.cloned.1.call-done = f32[16,1024]{1,0:T(8,128)} async-done(((f32[16,8192]{1,0:T(8,128)}), f32[16,1024]{1,0:T(8,128)}) %reduce-scatter.6.cloned.1.call-update) | async-done | bytes 65552 | tf_op jit(solution)/shard_map/reduce_scatter | solution.py:123
  137.1 14.2 %all_gather.15 = bf16[16,8192]{1,0:T(8,128)(2,1)S(1)} all-gather(bf16[16,1024]{1,0:T(8,128)(2,1)S(1)} %multiply_convert_fusion.1), channel_id=1, replica_groups=mesh['grp'=2,'dp'=2,'kv'=4,'tp'=2] {'kv','tp'}, dimensions={1}, use_global_device_ids=true | all-gather | bytes 294912 | tf_op jit(solution)/shard_map/all_gather | solution.py:127
  151.3 5.2 %fusion.32 = f32[16,512]{1,0:T(8,128)} fusion(bf16[16,8192]{1,0:T(8,128)(2,1)S(1)} %all_gather.15, bf16[8192,512]{1,0:T(8,128)(2,1)} %param.49), kind=kOutput, calls=%fused_computation.74 | convolution fusion | flops 134217728 | bytes 8683520 | tf_op jit(solution)/shard_map/dot_general | solution.py:129
  156.5 8.3 %reduce-scatter.8.cloned.1.call-done = f32[8,512]{1,0:T(8,128)} async-done(((f32[16,512]{1,0:T(8,128)}), f32[8,512]{1,0:T(8,128)}) %reduce-scatter.8.cloned.1.call-update) | async-done | bytes 16400 | tf_op jit(solution)/shard_map/reduce_scatter | solution.py:128
  164.8 1.3 fusion.2
  (75 shorter events, 25.9 us)
Async XLA Ops:
  6.5 1.6 copy-start
  6.5 2.9 %copy-start.5 = (bf16[8,1024]{1,0:T(8,128)(2,1)S(1)}, bf16[8,1024]{1,0:T(8,128)(2,1)}, u32[]{:S(2)}) copy-start(bf16[8,1024]{1,0:T(8,128)(2,1)} %param.25) | copy-start | bytes 49156
  6.5 2.9 %copy-start.7 = (f32[1024]{0:T(1024)S(1)}, f32[1024]{0:T(1024)}, u32[]{:S(2)}) copy-start(f32[1024]{0:T(1024)} %param.26) | copy-start | bytes 12292
  6.5 42.8 %all-reduce.4.cloned.1.call-start = ((), (), s32[]{:S(2)}) async-start(), calls=%async_computation.6 | async-start | bytes 204800
  8.1 1.6 copy-start.1
  8.1 2.0 %copy-start.2 = (bf16[1024,512]{1,0:T(8,128)(2,1)S(1)}, bf16[1024,512]{1,0:T(8,128)(2,1)}, u32[]{:S(2)}) copy-start(bf16[1024,512]{1,0:T(8,128)(2,1)} %param.29) | copy-start | bytes 3145732
  9.8 1.3 copy-start.3
  9.8 1.5 copy-start.8
  9.8 16.6 %copy-start.10 = (f32[4,512]{1,0:T(4,128)S(1)}, f32[4,512]{1,0:T(4,128)}, u32[]{:S(2)}) copy-start(f32[4,512]{1,0:T(4,128)} %param.34) | copy-start | bytes 24580
  9.8 17.3 %copy-start.11 = (f32[4,512]{1,0:T(4,128)S(1)}, f32[4,512]{1,0:T(4,128)}, u32[]{:S(2)}) copy-start(f32[4,512]{1,0:T(4,128)} %param.33) | copy-start | bytes 24580
  11.4 0.6 copy-start.6
  12.1 52.1 %copy-start.4 = (f32[2,16,64,128]{3,2,1,0:T(8,128)S(1)}, f32[2,16,64,128]{3,2,1,0:T(8,128)}, u32[]{:S(2)}) copy-start(f32[2,16,64,128]{3,2,1,0:T(8,128)} %param.44) | copy-start | bytes 3145732
  12.1 81.0 %reduce-scatter.4.cloned.1.call-start = ((), (), s32[]{:S(2)}) async-start(), calls=%async_computation.3 | async-start | bytes 49152 | tf_op jit(solution)/shard_map/reduce_scatter | solution.py:108
  58.3 7.7 %copy-start.9 = (f32[2]{0:T(128)S(1)}, f32[2]{0:T(128)}, u32[]{:S(2)}) copy-start(f32[2]{0:T(128)} %fusion.19) | copy-start | bytes 28
  58.3 11.2 %copy-start.12 = (f32[1024]{0:T(1024)S(1)}, f32[1024]{0:T(1024)}, u32[]{:S(2)}) copy-start(f32[1024]{0:T(1024)} %param.45) | copy-start | bytes 12292
  61.1 32.1 %copy-start.13 = (f32[512]{0:T(512)S(1)}, f32[512]{0:T(512)}, u32[]{:S(2)}) copy-start(f32[512]{0:T(512)} %param.47) | copy-start | bytes 6148
  85.5 50.8 %reduce-scatter.6.cloned.1.call-start = ((), (), s32[]{:S(2)}) async-start(), calls=%async_computation.4 | async-start | bytes 589824 | tf_op jit(solution)/shard_map/reduce_scatter | solution.py:123
  103.6 61.2 %reduce-scatter.8.cloned.1.call-start = ((), (), s32[]{:S(2)}) async-start(), calls=%async_computation.5 | async-start | bytes 49152 | tf_op jit(solution)/shard_map/reduce_scatter | solution.py:128
Sparse Core Ops, SparseCore 0:
  12.2 37.1 all-reduce.3
  85.6 7.5 reduce-scatter.3
  103.7 32.4 reduce-scatter.5
  156.6 8.0 reduce-scatter.7
where the time goes:
time: 174 us; the launch traced here: 173 us
  blocking collectives  67.6 us (39%)
  waiting for transfers between devices  36.2 us (21%)
  matrix products  19.4 us (11%)
  local copies, waits for them, and re-layouts  18.1 us (10%)
  other arithmetic  17.4 us (10%)
  between operations  13.9 us (8%)
    psum x1, blocking collectives, per_device(): sq_sum = lax.psum(row_sq, ('kv', 'tp'))  14.8 us
    all_gather x1, blocking collectives, per_device(): hidden_units = lax.all_gather(unit_share, ('kv', 'tp'), axis=1, tiled=True)  14.2 us
    unnamed x1, blocking collectives  14.1 us
    all_gather x1, blocking collectives, per_device(): lax.all_gather(normed, 'kv', axis=0, tiled=True)  13.2 us
    reduce_scatter x1, waiting for transfers between devices, per_device(): lax.psum_scatter(partial_value, ('kv', 'tp'), scatter_dimension=1, tiled=...  13.2 us
    reduce_scatter x1, waiting for transfers between devices, per_device(): lax.psum_scatter(jnp.dot(hidden_units, w_down, preferred_element_type=jnp...  8.27 us
    reduce_scatter x1, waiting for transfers between devices, per_device(): mixed_in = lax.psum_scatter(products, 'tp', scatter_dimension=1, tiled=True)  7.61 us
    unnamed x32, local copies, waits for them, and re-layouts  7.41 us
  transfers between devices with their start and end apart: 4, of which 4 were waited for; matrix products, arithmetic and copies ran while one was open for 9% of the time, Pallas kernels for 0%

commit v1 on v0

--- a/solution.py
+++ b/solution.py
@@ -1,6 +1,10 @@
+import functools
+
 import jax
 import jax.numpy as jnp
 from jax import lax
+from jax.experimental import pallas as pl
+from jax.experimental.pallas import tpu as pltpu
 from jax.sharding import PartitionSpec as P
 
 D = 4096
@@ -134,9 +138,475 @@
     return (hidden.astype(jnp.float32) + lowered).astype(jnp.bfloat16)
 
 
+MESH = pl.DeviceIdType.MESH
+LANES = 128
+F32 = jnp.float32
+BF16 = jnp.bfloat16
+
+(
+    INPUTS,
+    GAIN_IN,
+    W_GATE,
+    W_INPUT,
+    W_BPROJ,
+    W_CPROJ,
+    W_STEP,
+    CONV_INPUT,
+    CONV_BPROJ,
+    CONV_CPROJ,
+    TAIL_INPUT,
+    TAIL_BPROJ,
+    TAIL_CPROJ,
+    STEP_BIAS,
+    DECAY_LOG,
+    BLOCK_INPUT,
+    BLOCK_BPROJ,
+    BLOCK_STEP,
+    LENGTHS,
+    STATE,
+    GAIN_MIX,
+    W_OUT,
+    GAIN_MLP,
+    W_UP,
+    W_DOWN,
+) = NAMES = range(25)
+EARLY = (
+    INPUTS, GAIN_IN, W_STEP, W_GATE, W_INPUT, W_BPROJ, W_CPROJ,
+)
+MIDDLE = (
+    CONV_INPUT, CONV_BPROJ, CONV_CPROJ, TAIL_INPUT, TAIL_BPROJ, TAIL_CPROJ,
+    STEP_BIAS, DECAY_LOG, BLOCK_STEP, BLOCK_BPROJ, BLOCK_INPUT, STATE,
+    GAIN_MIX, W_OUT, GAIN_MLP,
+)
+LATE = (W_UP, W_DOWN)
+COPIED = EARLY + MIDDLE + LATE
+
+
+def send(source, target, send_sem, recv_sem, device):
+    copy = pltpu.make_async_remote_copy(
+        src_ref=source,
+        dst_ref=target,
+        send_sem=send_sem,
+        recv_sem=recv_sem,
+        device_id=device,
+        device_id_type=MESH,
+    )
+    copy.start()
+    return copy
+
+
+def taps(history, weights, newest):
+    past = history.astype(F32)
+    summed = weights[TAPS - 1 :] * newest
+    for offset in range(TAPS - 1):
+        summed = summed + weights[offset : offset + 1] * past[offset : offset + 1]
+    return summed * lax.logistic(summed)
+
+
+def fused(sizes, *refs):
+    kv, tp, dp = sizes
+    hbm = dict(zip(NAMES, refs[: len(NAMES)]))
+    out_ref = refs[len(NAMES)]
+    rest = list(refs[len(NAMES) + 1 :])
+    vm = dict(zip(COPIED, rest[: len(COPIED)]))
+    (
+        a_send, a_recv, g_buf, p_send, p_recv, h_buf, q_buf, u_send, u_recv, r_send, r_recv, own_sum,
+        units, l_send, l_recv,
+        local_sem, a_ss, a_rs, g_ss, g_rs, p_ss, p_rs, h_ss, h_rs, q_ss, q_rs, u_ss, u_rs,
+        r_ss, r_rs, n_ss, n_rs, f_ss, f_rs, l_ss, l_rs,
+    ) = rest[len(COPIED) :]
+    me_kv, me_tp, me_dp = lax.axis_index("kv"), lax.axis_index("tp"), lax.axis_index("dp")
+    me_unit = me_kv * tp + me_tp
+
+    def kv_peer(j):
+        return lax.rem(me_kv + j, kv)
+
+    def tp_peer(q):
+        return lax.rem(me_tp + q, tp)
+
+    def dp_peer(d):
+        return lax.rem(me_dp + d, dp)
+
+    pairs = [(j, q) for j in range(kv) for q in range(tp) if j or q]
+    far_first = sorted(range(kv), key=lambda j: -min(j, kv - j))
+    near_first = [j for j in reversed(far_first) if j]
+
+    barrier = pltpu.get_barrier_semaphore()
+    for j, q in pairs:
+        pl.semaphore_signal(
+            barrier, inc=1, device_id={"kv": kv_peer(j), "tp": tp_peer(q)}, device_id_type=MESH
+        )
+    for d in range(1, dp):
+        pl.semaphore_signal(barrier, inc=1, device_id={"dp": dp_peer(d)}, device_id_type=MESH)
+
+    local = {
+        name: pltpu.make_async_copy(hbm[name], vm[name], local_sem.at[index])
+        for index, name in enumerate(COPIED)
+    }
+    for name in EARLY + MIDDLE:
+        local[name].start()
+    pending = []
+
+    local[INPUTS].wait()
+    local[GAIN_IN].wait()
+    stream = vm[INPUTS][...].astype(F32)
+    rows = stream.shape[0]
+    seqs = rows // kv
+    scaled = (stream * vm[GAIN_IN][...]).astype(BF16)
+    squares = jnp.sum(stream * stream, axis=1, keepdims=True)
+    offsets = {}
+    at = 0
+    for name in (W_GATE, W_INPUT, W_BPROJ, W_CPROJ, W_STEP):
+        width = vm[name].shape[1]
+        offsets[name] = at
+        local[name].wait()
+        piece = jnp.dot(scaled, vm[name][...], preferred_element_type=F32)
+        for k in range(kv):
+            a_send[k, :, at : at + width] = piece[k * seqs : (k + 1) * seqs]
+        at += -(-width // LANES) * LANES
+    wide_squares = jnp.broadcast_to(squares, (rows, LANES))
+    for k in range(kv):
+        a_send[k, :, at : at + LANES] = wide_squares[k * seqs : (k + 1) * seqs]
+    for name in LATE:
+        local[name].start()
+    pl.semaphore_wait(barrier, len(pairs) + dp - 1)
+    copies = [
+        send(a_send.at[kv_peer(j)], a_recv.at[j - 1], a_ss.at[j - 1], a_rs.at[j - 1], {"kv": kv_peer(j)})
+        for j in far_first
+        if j
+    ]
+
+    for name in MIDDLE[:-3]:
+        local[name].wait()
+    heads = vm[STEP_BIAS].shape[1]
+    groups = vm[W_BPROJ].shape[1] // D_STATE
+    per_group = heads // groups
+    channels = heads * HEAD_DIM
+    block = vm[BLOCK_STEP].shape[1]
+    head_eye = lax.broadcasted_iota(jnp.int32, (heads, heads), 0) == lax.broadcasted_iota(
+        jnp.int32, (heads, heads), 1
+    )
+    eye = head_eye.astype(F32)
+
+    def column(row):
+        return jnp.sum(jnp.where(head_eye, row, 0.0), axis=1, keepdims=True)
+
+    later_than = (
+        lax.broadcasted_iota(jnp.int32, (block, block), 0)
+        > lax.broadcasted_iota(jnp.int32, (block, block), 1)
+    ).astype(F32)
+    positions = lax.broadcasted_iota(jnp.int32, (heads, block), 1)
+    decay_rate = column(-jnp.exp(vm[DECAY_LOG][...]))
+    prepared = []
+    for b in range(seqs):
+        live = positions < hbm[LENGTHS][b]
+        steps = lax.dot_general(
+            eye,
+            vm[BLOCK_STEP][b],
+            (((1,), (1,)), ((), ())),
+            precision=lax.Precision.HIGHEST,
+            preferred_element_type=F32,
+        )
+        masked = jnp.where(live, steps, 0.0)
+        later = jnp.dot(
+            masked, later_than, precision=lax.Precision.HIGHEST, preferred_element_type=F32
+        )
+        prepared.append((live, steps, later, jnp.sum(masked, axis=1, keepdims=True)))
+    own_head = lax.broadcasted_iota(jnp.int32, (heads, channels), 0) == (
+        lax.broadcasted_iota(jnp.int32, (heads, channels), 1) // HEAD_DIM
+    )
+    own_group = (lax.broadcasted_iota(jnp.int32, (heads, groups * D_STATE), 0) // per_group) == (
+        lax.broadcasted_iota(jnp.int32, (heads, groups * D_STATE), 1) // D_STATE
+    )
+
+    projected = a_send[me_kv]
+    for copy, j in zip(copies, [j for j in far_first if j]):
+        copy.wait_recv()
+        projected = projected + a_recv[j - 1]
+    pending += copies
+    features = vm[INPUTS].shape[1] * kv
+    inverse = lax.rsqrt(projected[:, at : at + 1] / features + EPS)
+
+    def part(name):
+        start = offsets[name]
+        return projected[:, start : start + vm[name].shape[1]] * inverse
+
+    gate_pre, value_pre, b_pre, c_pre, step_pre = [
+        part(name) for name in (W_GATE, W_INPUT, W_BPROJ, W_CPROJ, W_STEP)
+    ]
+    biased = step_pre + vm[STEP_BIAS][...]
+    softened = jnp.maximum(biased, 0.0) + jnp.log1p(jnp.exp(-jnp.abs(biased)))
+    mixed_rows = []
+    for b in range(seqs):
+        live, steps, later, total_steps = prepared[b]
+        current = taps(vm[TAIL_INPUT][b], vm[CONV_INPUT][...], value_pre[b : b + 1])
+        b_now = taps(vm[TAIL_BPROJ][b], vm[CONV_BPROJ][...], b_pre[b : b + 1])
+        c_now = taps(vm[TAIL_CPROJ][b], vm[CONV_CPROJ][...], c_pre[b : b + 1])
+        step_size = column(softened[b : b + 1])
+        c_spread = jnp.where(own_group, c_now, 0.0)
+        scores = lax.dot_general(
+            c_spread.astype(BF16),
+            vm[BLOCK_BPROJ][b],
+            (((1,), (1,)), ((), ())),
+            preferred_element_type=F32,
+        )
+        decays = jnp.where(live, jnp.exp(decay_rate * (step_size + later)), 0.0)
+        weights = (decays * scores * steps).astype(BF16)
+        inner = jnp.dot(weights, vm[BLOCK_INPUT][b], preferred_element_type=F32)
+        own_score = jnp.sum(c_spread * b_now, axis=1, keepdims=True)
+        carried = jnp.exp(decay_rate * (step_size + total_steps))
+        c_heads = sum(
+            c_spread[:, g * D_STATE : (g + 1) * D_STATE] for g in range(groups)
+        )
+        readout = lax.dot_general(
+            c_heads,
+            vm[STATE][b].reshape(channels, D_STATE),
+            (((1,), (1,)), ((), ())),
+            precision=lax.Precision.HIGHEST,
+            preferred_element_type=F32,
+        )
+        terms = inner + (step_size * own_score) * current + carried * readout
+        mixed_rows.append(jnp.sum(jnp.where(own_head, terms, 0.0), axis=0, keepdims=True))
+    mixed = jnp.concatenate(mixed_rows, axis=0) * (gate_pre * lax.logistic(gate_pre))
+    local[GAIN_MIX].wait()
+    g_buf[me_kv, :, :channels] = mixed * vm[GAIN_MIX][...]
+    g_buf[me_kv, :, channels:] = jnp.broadcast_to(
+        jnp.sum(mixed * mixed, axis=1, keepdims=True), (seqs, LANES)
+    )
+    copies = [
+        send(g_buf.at[me_kv], g_buf.at[me_kv], g_ss.at[j - 1], g_rs.at[j - 1], {"kv": kv_peer(j)})
+        for j in far_first
+        if j
+    ]
+    local[W_OUT].wait()
+    local[GAIN_MLP].wait()
+    for copy in copies:
+        copy.wait_recv()
+    pending += copies
+
+    gathered = jnp.concatenate([g_buf[k] for k in range(kv)], axis=0)
+    unscaled = gathered[:, :channels].astype(BF16)
+    share = vm[W_OUT].shape[1] // tp
+    for q in range(tp):
+        p_send[q, :, :share] = jnp.dot(
+            unscaled, vm[W_OUT][:, q * share : (q + 1) * share], preferred_element_type=F32
+        )
+        p_send[q, :, share:] = gathered[:, channels:]
+    copies = [
+        send(p_send.at[tp_peer(q)], p_recv.at[q - 1], p_ss.at[q - 1], p_rs.at[q - 1], {"tp": tp_peer(q)})
+        for q in range(1, tp)
+    ]
+    residual = stream[:, :share]
+    for q in range(1, tp):
+        residual = jnp.where(me_tp == q, stream[:, q * share : (q + 1) * share], residual)
+    summed = p_send[me_tp]
+    for q, copy in enumerate(copies):
+        copy.wait_recv()
+        summed = summed + p_recv[q]
+    pending += copies
+    mixed_in = summed[:, :share] * lax.rsqrt(summed[:, share : share + 1] / (channels * tp) + EPS)
+    hidden = (residual + mixed_in).astype(BF16).astype(F32)
+    h_buf[me_dp] = hidden
+    copies = [
+        send(h_buf.at[me_dp], h_buf.at[me_dp], h_ss.at[d - 1], h_rs.at[d - 1], {"dp": dp_peer(d)})
+        for d in range(1, dp)
+    ]
+    local[W_UP].wait()
+    for copy in copies:
+        copy.wait_recv()
+    pending += copies
+
+    whole_rows = jnp.concatenate([h_buf[d] for d in range(dp)], axis=0)
+    lifted = (whole_rows * vm[GAIN_MLP][...]).astype(BF16)
+    all_rows = rows * dp
+    row_eye = lax.broadcasted_iota(jnp.int32, (all_rows, q_buf.shape[2]), 0) == (
+        lax.broadcasted_iota(jnp.int32, (all_rows, q_buf.shape[2]), 1)
+    )
+    row_sq = jnp.sum(whole_rows * whole_rows, axis=1, keepdims=True)
+    q_buf[0] = jnp.sum(jnp.where(row_eye, row_sq, 0.0), axis=0, keepdims=True)
+    q_copies = [
+        send(
+            q_buf.at[0],
+            q_buf.at[slot],
+            q_ss.at[slot - 1],
+            q_rs.at[slot - 1],
+            {"kv": kv_peer(j), "tp": tp_peer(q)},
+        )
+        for slot, (j, q) in enumerate(pairs, 1)
+    ]
+    unit_share = vm[W_UP].shape[1] // (kv * tp)
+
+    def raised(j, q):
+        chunk = kv_peer(j) * tp + tp_peer(q)
+        columns = pl.ds(pl.multiple_of(chunk * unit_share, LANES), unit_share)
+        return jnp.dot(lifted, vm[W_UP][:, columns], preferred_element_type=F32)
+
+    u_copies = {}
+    for j in far_first:
+        for q in range(1, tp):
+            u_send[q - 1, j] = raised(j, q)
+            u_copies[j, q] = send(
+                u_send.at[q - 1, j],
+                u_recv.at[q - 1, j],
+                u_ss.at[q - 1, j],
+                u_rs.at[q - 1, j],
+                {"tp": tp_peer(q)},
+            )
+    r_copies = {}
+    for j in far_first:
+        total = raised(j, 0)
+        for q in range(1, tp):
+            u_copies[j, q].wait_recv()
+            total = total + u_recv[q - 1, j]
+        if j:
+            r_send[j - 1] = total.astype(BF16)
+            r_copies[j] = send(
+                r_send.at[j - 1], r_recv.at[j - 1], r_ss.at[j - 1], r_rs.at[j - 1], {"kv": kv_peer(j)}
+            )
+        else:
+            own_sum[...] = total
+    pending += list(u_copies.values()) + list(r_copies.values()) + q_copies
+    sq_row = q_buf[0]
+    for slot, copy in enumerate(q_copies, 1):
+        copy.wait_recv()
+        sq_row = sq_row + q_buf[slot]
+    sq_sum = jnp.sum(jnp.where(row_eye, sq_row, 0.0), axis=1, keepdims=True)
+    inverse_mlp = lax.rsqrt(sq_sum / features + EPS)
+    shares = own_sum[...]
+    for j in near_first:
+        r_copies[j].wait_recv()
+        shares = shares + r_recv[j - 1].astype(F32)
+    active = jnp.maximum(shares * inverse_mlp, 0.0)
+    units[me_unit] = (active * active).astype(BF16)
+
+    n_copies = {}
+    for j in far_first:
+        if j:
+            n_copies[j] = send(
+                units.at[me_unit], units.at[me_unit], n_ss.at[j - 1], n_rs.at[j - 1], {"kv": kv_peer(j)}
+            )
+    f_copies = {}
+
+    def forward(j):
+        for q in range(1, tp):
+            chunk = lax.rem(me_kv + kv - j, kv) * tp + me_tp
+            f_copies[j, q] = send(
+                units.at[chunk], units.at[chunk], f_ss.at[q - 1, j], f_rs.at[q - 1, j], {"tp": tp_peer(q)}
+            )
+
+    def lower(j, q):
+        chunk = lax.rem(me_kv + kv - j, kv) * tp + lax.rem(me_tp + tp - q, tp)
+        span = pl.ds(pl.multiple_of(chunk * unit_share, LANES), unit_share)
+        return jnp.dot(units[chunk], vm[W_DOWN][span, :], preferred_element_type=F32)
+
+    forward(0)
+    local[W_DOWN].wait()
+    lowered = lower(0, 0)
+    for q in range(1, tp):
+        f_copies[0, q].wait_recv()
+        lowered = lowered + lower(0, q)
+    for j in near_first:
+        n_copies[j].wait_recv()
+        forward(j)
+        lowered = lowered + lower(j, 0)
+    for j in near_first:
+        for q in range(1, tp):
+            f_copies[j, q].wait_recv()
+            lowered = lowered + lower(j, q)
+    pending += list(n_copies.values()) + list(f_copies.values())
+
+    for d in range(dp):
+        l_send[d] = lowered[d * rows : (d + 1) * rows]
+    copies = [
+        send(l_send.at[dp_peer(d)], l_recv.at[d - 1], l_ss.at[d - 1], l_rs.at[d - 1], {"dp": dp_peer(d)})
+        for d in range(1, dp)
+    ]
+    for copy in pending:
+        copy.wait_send()
+    result = h_buf[me_dp] + l_send[me_dp]
+    for d, copy in enumerate(copies):
+        copy.wait_recv()
+        result = result + l_recv[d]
+    out_ref[...] = result.astype(BF16)
+    for copy in copies:
+        copy.wait_send()
+
+
+def fused_device(sizes, *args):
+    kv, tp, dp = sizes
+    named = dict(zip(NAMES, args))
+    for name in (GAIN_IN, STEP_BIAS, DECAY_LOG, GAIN_MIX, GAIN_MLP):
+        named[name] = named[name].reshape(1, -1)
+    rows = named[INPUTS].shape[0]
+    seqs = rows // kv
+    pads = [
+        -(-named[name].shape[1] // LANES) * LANES
+        for name in (W_GATE, W_INPUT, W_BPROJ, W_CPROJ, W_STEP)
+    ]
+    wide = sum(pads) + LANES
+    channels = named[W_GATE].shape[1]
+    share = named[W_OUT].shape[1] // tp
+    all_rows = rows * dp
+    unit_share = named[W_UP].shape[1] // (kv * tp)
+    columns = named[W_DOWN].shape[1]
+    row_lanes = -(-all_rows // LANES) * LANES
+    dma = pltpu.SemaphoreType.DMA
+    scratch = [pltpu.VMEM(named[name].shape, named[name].dtype) for name in COPIED] + [
+        pltpu.VMEM((kv, seqs, wide), F32),
+        pltpu.VMEM((kv - 1, seqs, wide), F32),
+        pltpu.VMEM((kv, seqs, channels + LANES), F32),
+        pltpu.VMEM((tp, rows, share + LANES), F32),
+        pltpu.VMEM((tp - 1, rows, share + LANES), F32),
+        pltpu.VMEM((dp, rows, share), F32),
+        pltpu.VMEM((kv * tp, 1, row_lanes), F32),
+        pltpu.VMEM((tp - 1, kv, all_rows, unit_share), F32),
+        pltpu.VMEM((tp - 1, kv, all_rows, unit_share), F32),
+        pltpu.VMEM((kv - 1, all_rows, unit_share), BF16),
+        pltpu.VMEM((kv - 1, all_rows, unit_share), BF16),
+        pltpu.VMEM((all_rows, unit_share), F32),
+        pltpu.VMEM((kv * tp, all_rows, unit_share), BF16),
+        pltpu.VMEM((dp, rows, columns), F32),
+        pltpu.VMEM((dp - 1, rows, columns), F32),
+        dma((len(COPIED),)),
+        dma((kv - 1,)), dma((kv - 1,)),
+        dma((kv - 1,)), dma((kv - 1,)),
+        dma((tp - 1,)), dma((tp - 1,)),
+        dma((dp - 1,)), dma((dp - 1,)),
+        dma((kv * tp - 1,)), dma((kv * tp - 1,)),
+        dma((tp - 1, kv)), dma((tp - 1, kv)),
+        dma((kv - 1,)), dma((kv - 1,)),
+        dma((kv - 1,)), dma((kv - 1,)),
+        dma((tp - 1, kv)), dma((tp - 1, kv)),
+        dma((dp - 1,)), dma((dp - 1,)),
+    ]
+    spaces = [
+        pl.BlockSpec(memory_space=pltpu.SMEM if name == LENGTHS else pl.ANY) for name in NAMES
+    ]
+    return pl.pallas_call(
+        functools.partial(fused, sizes),
+        out_shape=jax.ShapeDtypeStruct((rows, columns), BF16),
+        in_specs=spaces,
+        out_specs=pl.BlockSpec(memory_space=pltpu.VMEM),
+        scratch_shapes=scratch,
+        compiler_params=pltpu.CompilerParams(
+            collective_id=0, has_side_effects=True, vmem_limit_bytes=60 * 1024 * 1024
+        ),
+    )(*[named[name] for name in NAMES])
+
+
+def choose(sizes, *args):
+    kv, tp, _ = sizes
+    named = dict(zip(NAMES, args))
+    pieces = (named[W_UP].shape[1] // (kv * tp), named[W_OUT].shape[1] // tp)
+    if min(sizes) > 1 and all(piece % LANES == 0 for piece in pieces):
+        return fused_device(sizes, *args)
+    return per_device(*args)
+
+
 def solution(mesh):
+    sizes = tuple(mesh.shape[axis] for axis in ("kv", "tp", "dp"))
     return jax.shard_map(
-        per_device,
+        functools.partial(choose, sizes),
         mesh=mesh,
         in_specs=(
             P(("grp", "dp"), "kv"),

time: 174 us -> 43.4 us (0.25)
  blocking collectives: 67.6 us -> 0 us
  waiting for transfers between devices: 36.2 us -> 0 us
  Pallas kernels: 0 us -> 34.6 us
  matrix products: 19.4 us -> 0 us
  other arithmetic: 17.4 us -> 0 us
  between operations: 13.9 us -> 0.01 us
  local copies, waits for them, and re-layouts: 18.1 us -> 8.25 us
    all_gather x4 -> x0, blocking collectives: 36.1 us -> none  [the longest x1 14.2 us: per_device(): hidden_units = lax.all_gather(unit_share, ('kv', 'tp'), axis=1, tiled=True)]
    pallas_call x0 -> x1, Pallas kernels: none -> 34.6 us  [fused_device(): pl.pallas_call(functools.partial(fused, sizes), out_shape=jax.ShapeDtypeS...]
    reduce_scatter x3 -> x0, waiting for transfers between devices: 29.1 us -> none  [the longest x1 13.2 us: per_device(): lax.psum_scatter(partial_value, ('kv', 'tp'), scatter_dimension=1, tiled=...]
    dot_general x11 -> x0, matrix products: 19.4 us -> none  [the longest x1 5.38 us: per_device(): jnp.dot(all_lifted, w_up, preferred_element_type=jnp.float32)]
    psum x2 -> x0, blocking collectives: 17.3 us -> none  [the longest x1 14.8 us: per_device(): sq_sum = lax.psum(row_sq, ('kv', 'tp'))]
    unnamed x1 -> x0, blocking collectives: 14.1 us -> none
    unnamed x5 -> x0, waiting for transfers between devices: 7.12 us -> none
    convert_element_type x7 -> x0, other arithmetic: 6.77 us -> none  [the longest x1 1.53 us: per_device(): c_now.astype(jnp.bfloat16).reshape(seq_count, group_count, D_STATE)]
  transfers between devices with their start and end apart: 4 -> 0, of which waited for: 4 -> 0; matrix products, arithmetic and copies ran while one was open for 9% -> 0% of each run, Pallas kernels for 0% -> 0%
where the time goes in v1:
time: 43.4 us; the launch traced here: 42.8 us
  Pallas kernels  34.6 us (80%)
  local copies, waits for them, and re-layouts  8.25 us (19%)
    pallas_call x1, Pallas kernels, fused_device(): pl.pallas_call(functools.partial(fused, sizes), out_shape=jax.ShapeDtypeS...  34.6 us
    unnamed x6, local copies, waits for them, and re-layouts  8.25 us

profile of v1, /device:TPU:0, one launch (start us, length us, event | category | flops | bytes accessed | tf_op | source)
XLA Modules:
  0.0 42.8 jit_solution(14262532522547195243)
XLA Ops:
  0.0 1.3 %copy.28.refs_11_ = bf16[2,3,512]{2,1,0:T(4,128)(2,1)} copy(bf16[2,3,512]{2,0,1:T(2,128)(2,1)} %param.36) | data formatting | bytes 12288 | tf_op args[11]
  1.3 1.3 %copy.29.refs_12_ = bf16[2,3,512]{2,1,0:T(4,128)(2,1)} copy(bf16[2,3,512]{2,0,1:T(2,128)(2,1)} %param.37) | data formatting | bytes 12288 | tf_op args[12]
  2.6 1.3 %copy.27.refs_10_ = bf16[2,3,1024]{2,1,0:T(4,128)(2,1)} copy(bf16[2,3,1024]{2,0,1:T(2,128)(2,1)} %param.35) | data formatting | bytes 24576 | tf_op args[10]
  3.9 1.5 %copy.30.refs_17_ = f32[2,128,16]{2,1,0:T(8,128)} copy(f32[2,128,16]{1,2,0:T(8,128)} %param.42) | data formatting | bytes 32768 | tf_op args[17]
  5.4 1.6 %copy.26.refs_6_ = bf16[1024,16]{1,0:T(8,128)(2,1)} copy(bf16[1024,16]{0,1:T(8,128)(2,1)} %param.31) | data formatting | bytes 65536 | tf_op args[6]
  7.0 34.6 %shard_map.235 = bf16[8,512]{1,0:T(8,128)(2,1)} custom-call(bf16[8,1024]{1,0:T(8,128)(2,1)} %refs_0_.1, f32[1,1024]{1,0:T(1,128)} %bitcast.5, bf16[1024,1024]{1,0:T(8,128)(2,1)} %refs_2_.1, bf16[1024,1024]{1,0:T(8,128)(2,1)} %refs_3_.1, bf16[1024,512]{1,0:T(8,128)(2,1)} %refs_4_.1, bf16[1024,512]{1,0:T(8,128)(2,1)} %refs_5_.1, ...), custom_call_target="tpu_custom_call" | custom-call | tf_op jit(solution)/shard_map/pallas_call | solution.py:585
  41.5 1.3 %copy.32 = bf16[8,512]{1,0:T(8,128)(2,1)} copy(bf16[8,512]{1,0:T(8,128)(2,1)} %shard_map.235) | data formatting | bytes 16384

commit v2 on v1

--- a/solution.py
+++ b/solution.py
@@ -196,10 +196,9 @@
 
 
 def taps(history, weights, newest):
-    past = history.astype(F32)
     summed = weights[TAPS - 1 :] * newest
     for offset in range(TAPS - 1):
-        summed = summed + weights[offset : offset + 1] * past[offset : offset + 1]
+        summed = summed + weights[offset : offset + 1] * history[offset].astype(F32)
     return summed * lax.logistic(summed)
 
 
@@ -243,7 +242,7 @@
         name: pltpu.make_async_copy(hbm[name], vm[name], local_sem.at[index])
         for index, name in enumerate(COPIED)
     }
-    for name in EARLY + MIDDLE:
+    for name in EARLY:
         local[name].start()
     pending = []
 
@@ -254,13 +253,21 @@
     seqs = rows // kv
     scaled = (stream * vm[GAIN_IN][...]).astype(BF16)
     squares = jnp.sum(stream * stream, axis=1, keepdims=True)
-    offsets = {}
+    spans = {}
     at = 0
     for name in (W_GATE, W_INPUT, W_BPROJ, W_CPROJ, W_STEP):
-        width = vm[name].shape[1]
-        offsets[name] = at
+        width = vm[name].shape[name != W_STEP]
+        spans[name] = at, at + width
         local[name].wait()
-        piece = jnp.dot(scaled, vm[name][...], preferred_element_type=F32)
+        if name == W_GATE:
+            for other in MIDDLE:
+                local[other].start()
+        piece = lax.dot_general(
+            scaled,
+            vm[name][...],
+            (((1,), (int(name == W_STEP),)), ((), ())),
+            preferred_element_type=F32,
+        )
         for k in range(kv):
             a_send[k, :, at : at + width] = piece[k * seqs : (k + 1) * seqs]
         at += -(-width // LANES) * LANES
@@ -282,11 +289,10 @@
     groups = vm[W_BPROJ].shape[1] // D_STATE
     per_group = heads // groups
     channels = heads * HEAD_DIM
-    block = vm[BLOCK_STEP].shape[1]
+    block = vm[BLOCK_STEP].shape[2]
     head_eye = lax.broadcasted_iota(jnp.int32, (heads, heads), 0) == lax.broadcasted_iota(
         jnp.int32, (heads, heads), 1
     )
-    eye = head_eye.astype(F32)
 
     def column(row):
         return jnp.sum(jnp.where(head_eye, row, 0.0), axis=1, keepdims=True)
@@ -300,18 +306,15 @@
     prepared = []
     for b in range(seqs):
         live = positions < hbm[LENGTHS][b]
-        steps = lax.dot_general(
-            eye,
-            vm[BLOCK_STEP][b],
-            (((1,), (1,)), ((), ())),
-            precision=lax.Precision.HIGHEST,
-            preferred_element_type=F32,
-        )
+        steps = vm[BLOCK_STEP][b]
         masked = jnp.where(live, steps, 0.0)
         later = jnp.dot(
             masked, later_than, precision=lax.Precision.HIGHEST, preferred_element_type=F32
         )
-        prepared.append((live, steps, later, jnp.sum(masked, axis=1, keepdims=True)))
+        state = vm[STATE][b].reshape(channels, D_STATE)
+        high = state.astype(BF16)
+        state_parts = jnp.concatenate([high, (state - high.astype(F32)).astype(BF16)], axis=1)
+        prepared.append((live, steps, later, jnp.sum(masked, axis=1, keepdims=True), state_parts))
     own_head = lax.broadcasted_iota(jnp.int32, (heads, channels), 0) == (
         lax.broadcasted_iota(jnp.int32, (heads, channels), 1) // HEAD_DIM
     )
@@ -328,8 +331,7 @@
     inverse = lax.rsqrt(projected[:, at : at + 1] / features + EPS)
 
     def part(name):
-        start = offsets[name]
-        return projected[:, start : start + vm[name].shape[1]] * inverse
+        return projected[:, spans[name][0] : spans[name][1]] * inverse
 
     gate_pre, value_pre, b_pre, c_pre, step_pre = [
         part(name) for name in (W_GATE, W_INPUT, W_BPROJ, W_CPROJ, W_STEP)
@@ -337,11 +339,12 @@
     biased = step_pre + vm[STEP_BIAS][...]
     softened = jnp.maximum(biased, 0.0) + jnp.log1p(jnp.exp(-jnp.abs(biased)))
     mixed_rows = []
+    all_current = taps(vm[TAIL_INPUT], vm[CONV_INPUT][...], value_pre)
+    all_b = taps(vm[TAIL_BPROJ], vm[CONV_BPROJ][...], b_pre)
+    all_c = taps(vm[TAIL_CPROJ], vm[CONV_CPROJ][...], c_pre)
     for b in range(seqs):
-        live, steps, later, total_steps = prepared[b]
-        current = taps(vm[TAIL_INPUT][b], vm[CONV_INPUT][...], value_pre[b : b + 1])
-        b_now = taps(vm[TAIL_BPROJ][b], vm[CONV_BPROJ][...], b_pre[b : b + 1])
-        c_now = taps(vm[TAIL_CPROJ][b], vm[CONV_CPROJ][...], c_pre[b : b + 1])
+        live, steps, later, total_steps, state_parts = prepared[b]
+        current, b_now, c_now = all_current[b : b + 1], all_b[b : b + 1], all_c[b : b + 1]
         step_size = column(softened[b : b + 1])
         c_spread = jnp.where(own_group, c_now, 0.0)
         scores = lax.dot_general(
@@ -358,13 +361,19 @@
         c_heads = sum(
             c_spread[:, g * D_STATE : (g + 1) * D_STATE] for g in range(groups)
         )
-        readout = lax.dot_general(
-            c_heads,
-            vm[STATE][b].reshape(channels, D_STATE),
-            (((1,), (1,)), ((), ())),
-            precision=lax.Precision.HIGHEST,
-            preferred_element_type=F32,
-        )
+        c_high = c_heads.astype(BF16)
+        c_low = (c_heads - c_high.astype(F32)).astype(BF16)
+        both = jnp.concatenate(
+            [
+                jnp.concatenate([c_high, c_high], axis=1),
+                jnp.concatenate([c_low, jnp.zeros_like(c_low)], axis=1),
+            ],
+            axis=0,
+        )
+        doubled = lax.dot_general(
+            both, state_parts, (((1,), (1,)), ((), ())), preferred_element_type=F32
+        )
+        readout = doubled[:heads] + doubled[heads:]
         terms = inner + (step_size * own_score) * current + carried * readout
         mixed_rows.append(jnp.sum(jnp.where(own_head, terms, 0.0), axis=0, keepdims=True))
     mixed = jnp.concatenate(mixed_rows, axis=0) * (gate_pre * lax.logistic(gate_pre))
@@ -537,11 +546,16 @@
     named = dict(zip(NAMES, args))
     for name in (GAIN_IN, STEP_BIAS, DECAY_LOG, GAIN_MIX, GAIN_MLP):
         named[name] = named[name].reshape(1, -1)
+    named[W_STEP] = named[W_STEP].T
+    named[BLOCK_STEP] = named[BLOCK_STEP].transpose(0, 2, 1)
+    for name in (TAIL_INPUT, TAIL_BPROJ, TAIL_CPROJ):
+        named[name] = named[name].transpose(1, 0, 2)
     rows = named[INPUTS].shape[0]
     seqs = rows // kv
     pads = [
-        -(-named[name].shape[1] // LANES) * LANES
-        for name in (W_GATE, W_INPUT, W_BPROJ, W_CPROJ, W_STEP)
+        -(-width // LANES) * LANES
+        for width in [named[name].shape[1] for name in (W_GATE, W_INPUT, W_BPROJ, W_CPROJ)]
+        + [named[W_STEP].shape[0]]
     ]
     wide = sum(pads) + LANES
     channels = named[W_GATE].shape[1]

time: 43.4 us -> 35.6 us (0.82)
  local copies, waits for them, and re-layouts: 8.25 us -> 1.3 us
  Pallas kernels: 34.6 us -> 34 us
    unnamed x6 -> x1, local copies, waits for them, and re-layouts: 8.25 us -> 1.3 us
    pallas_call x1, Pallas kernels: 34.6 us -> 34 us  [fused_device(): pl.pallas_call(functools.partial(fused, sizes), out_shape=jax.ShapeDtypeS...]
where the time goes in v2:
time: 35.6 us; the launch traced here: 35.3 us
  Pallas kernels  34 us (96%)
  local copies, waits for them, and re-layouts  1.3 us (4%)
    pallas_call x1, Pallas kernels, fused_device(): pl.pallas_call(functools.partial(fused, sizes), out_shape=jax.ShapeDtypeS...  34 us
    unnamed x1, local copies, waits for them, and re-layouts  1.3 us

profile of v2, /device:TPU:0, one launch (start us, length us, event | category | flops | bytes accessed | tf_op | source)
XLA Modules:
  0.0 35.3 jit_solution(7080663038584614417)
XLA Ops:
  0.0 34.0 %shard_map.235 = bf16[8,512]{1,0:T(8,128)(2,1)} custom-call(bf16[8,1024]{1,0:T(8,128)(2,1)} %refs_0_.1, f32[1,1024]{1,0:T(1,128)} %bitcast.15, bf16[1024,1024]{1,0:T(8,128)(2,1)} %refs_2_.1, bf16[1024,1024]{1,0:T(8,128)(2,1)} %refs_3_.1, bf16[1024,512]{1,0:T(8,128)(2,1)} %refs_4_.1, bf16[1024,512]{1,0:T(8,128)(2,1)} %refs_5_.1, bf16[16,1024]{1,0:T(8,128)(2,1)} %bitcast.10, ...), custom_call_target="tpu_custom_call" | custom-call | tf_op jit(solution)/shard_map/pallas_call | solution.py:599
  34.0 1.3 %copy.27 = bf16[8,512]{1,0:T(8,128)(2,1)} copy(bf16[8,512]{1,0:T(8,128)(2,1)} %shard_map.235) | data formatting | bytes 16384

commit v3 on v2

--- a/solution.py
+++ b/solution.py
@@ -210,9 +210,9 @@
     vm = dict(zip(COPIED, rest[: len(COPIED)]))
     (
         a_send, a_recv, g_buf, p_send, p_recv, h_buf, q_buf, u_send, u_recv, r_send, r_recv, own_sum,
-        units, l_send, l_recv,
+        units, l_send, l_recv, s_send, s_recv, m_buf,
         local_sem, a_ss, a_rs, g_ss, g_rs, p_ss, p_rs, h_ss, h_rs, q_ss, q_rs, u_ss, u_rs,
-        r_ss, r_rs, n_ss, n_rs, f_ss, f_rs, l_ss, l_rs,
+        r_ss, r_rs, n_ss, n_rs, f_ss, f_rs, l_ss, l_rs, s_ss, s_rs, m_ss, m_rs,
     ) = rest[len(COPIED) :]
     me_kv, me_tp, me_dp = lax.axis_index("kv"), lax.axis_index("tp"), lax.axis_index("dp")
     me_unit = me_kv * tp + me_tp
@@ -257,11 +257,13 @@
     at = 0
     for name in (W_GATE, W_INPUT, W_BPROJ, W_CPROJ, W_STEP):
         width = vm[name].shape[name != W_STEP]
-        spans[name] = at, at + width
+        spans[name] = (at, at + width) if name != W_STEP else (0, width)
         local[name].wait()
         if name == W_GATE:
             for other in MIDDLE:
                 local[other].start()
+        if name == W_STEP:
+            at = 0
         piece = lax.dot_general(
             scaled,
             vm[name][...],
@@ -269,18 +271,25 @@
             preferred_element_type=F32,
         )
         for k in range(kv):
-            a_send[k, :, at : at + width] = piece[k * seqs : (k + 1) * seqs]
+            if name == W_STEP:
+                s_send[k, :, :width] = piece[k * seqs : (k + 1) * seqs]
+            else:
+                a_send[k, :, at : at + width] = piece[k * seqs : (k + 1) * seqs].astype(BF16)
         at += -(-width // LANES) * LANES
     wide_squares = jnp.broadcast_to(squares, (rows, LANES))
     for k in range(kv):
-        a_send[k, :, at : at + LANES] = wide_squares[k * seqs : (k + 1) * seqs]
+        s_send[k, :, at : at + LANES] = wide_squares[k * seqs : (k + 1) * seqs]
     for name in LATE:
         local[name].start()
     pl.semaphore_wait(barrier, len(pairs) + dp - 1)
+    others = [j for j in far_first if j]
     copies = [
         send(a_send.at[kv_peer(j)], a_recv.at[j - 1], a_ss.at[j - 1], a_rs.at[j - 1], {"kv": kv_peer(j)})
-        for j in far_first
-        if j
+        for j in others
+    ]
+    s_copies = [
+        send(s_send.at[kv_peer(j)], s_recv.at[j - 1], s_ss.at[j - 1], s_rs.at[j - 1], {"kv": kv_peer(j)})
+        for j in others
     ]
 
     for name in MIDDLE[:-3]:
@@ -322,16 +331,20 @@
         lax.broadcasted_iota(jnp.int32, (heads, groups * D_STATE), 1) // D_STATE
     )
 
-    projected = a_send[me_kv]
-    for copy, j in zip(copies, [j for j in far_first if j]):
+    projected = a_send[me_kv].astype(F32)
+    stepped = s_send[me_kv]
+    for copy, s_copy, j in zip(copies, s_copies, others):
         copy.wait_recv()
-        projected = projected + a_recv[j - 1]
-    pending += copies
+        s_copy.wait_recv()
+        projected = projected + a_recv[j - 1].astype(F32)
+        stepped = stepped + s_recv[j - 1]
+    pending += copies + s_copies
     features = vm[INPUTS].shape[1] * kv
-    inverse = lax.rsqrt(projected[:, at : at + 1] / features + EPS)
+    inverse = lax.rsqrt(stepped[:, at : at + 1] / features + EPS)
 
     def part(name):
-        return projected[:, spans[name][0] : spans[name][1]] * inverse
+        source = stepped if name == W_STEP else projected
+        return source[:, spans[name][0] : spans[name][1]] * inverse
 
     gate_pre, value_pre, b_pre, c_pre, step_pre = [
         part(name) for name in (W_GATE, W_INPUT, W_BPROJ, W_CPROJ, W_STEP)
@@ -378,14 +391,16 @@
         mixed_rows.append(jnp.sum(jnp.where(own_head, terms, 0.0), axis=0, keepdims=True))
     mixed = jnp.concatenate(mixed_rows, axis=0) * (gate_pre * lax.logistic(gate_pre))
     local[GAIN_MIX].wait()
-    g_buf[me_kv, :, :channels] = mixed * vm[GAIN_MIX][...]
-    g_buf[me_kv, :, channels:] = jnp.broadcast_to(
+    g_buf[me_kv] = (mixed * vm[GAIN_MIX][...]).astype(BF16)
+    m_buf[me_kv] = jnp.broadcast_to(
         jnp.sum(mixed * mixed, axis=1, keepdims=True), (seqs, LANES)
     )
     copies = [
         send(g_buf.at[me_kv], g_buf.at[me_kv], g_ss.at[j - 1], g_rs.at[j - 1], {"kv": kv_peer(j)})
-        for j in far_first
-        if j
+        for j in others
+    ] + [
+        send(m_buf.at[me_kv], m_buf.at[me_kv], m_ss.at[j - 1], m_rs.at[j - 1], {"kv": kv_peer(j)})
+        for j in others
     ]
     local[W_OUT].wait()
     local[GAIN_MLP].wait()
@@ -393,27 +408,32 @@
         copy.wait_recv()
     pending += copies
 
-    gathered = jnp.concatenate([g_buf[k] for k in range(kv)], axis=0)
-    unscaled = gathered[:, :channels].astype(BF16)
+    unscaled = jnp.concatenate([g_buf[k].astype(F32) for k in range(kv)], axis=0).astype(BF16)
+    partial_sq = jnp.concatenate([m_buf[k] for k in range(kv)], axis=0)
     share = vm[W_OUT].shape[1] // tp
-    for q in range(tp):
-        p_send[q, :, :share] = jnp.dot(
-            unscaled, vm[W_OUT][:, q * share : (q + 1) * share], preferred_element_type=F32
-        )
-        p_send[q, :, share:] = gathered[:, channels:]
-    copies = [
-        send(p_send.at[tp_peer(q)], p_recv.at[q - 1], p_ss.at[q - 1], p_rs.at[q - 1], {"tp": tp_peer(q)})
-        for q in range(1, tp)
-    ]
+
+    def product(q):
+        start = pl.multiple_of(tp_peer(q) * share, LANES)
+        return jnp.dot(unscaled, vm[W_OUT][:, pl.ds(start, share)], preferred_element_type=F32)
+
+    copies = []
+    for q in range(1, tp):
+        p_send[q - 1, :, :share] = product(q)
+        p_send[q - 1, :, share:] = partial_sq
+        copies.append(
+            send(p_send.at[q - 1], p_recv.at[q - 1], p_ss.at[q - 1], p_rs.at[q - 1], {"tp": tp_peer(q)})
+        )
+    summed = product(0)
     residual = stream[:, :share]
     for q in range(1, tp):
         residual = jnp.where(me_tp == q, stream[:, q * share : (q + 1) * share], residual)
-    summed = p_send[me_tp]
+    total_sq = partial_sq[:, :1]
     for q, copy in enumerate(copies):
         copy.wait_recv()
-        summed = summed + p_recv[q]
+        summed = summed + p_recv[q, :, :share]
+        total_sq = total_sq + p_recv[q, :, share : share + 1]
     pending += copies
-    mixed_in = summed[:, :share] * lax.rsqrt(summed[:, share : share + 1] / (channels * tp) + EPS)
+    mixed_in = summed * lax.rsqrt(total_sq / (channels * tp) + EPS)
     hidden = (residual + mixed_in).astype(BF16).astype(F32)
     h_buf[me_dp] = hidden
     copies = [
@@ -450,8 +470,9 @@
         columns = pl.ds(pl.multiple_of(chunk * unit_share, LANES), unit_share)
         return jnp.dot(lifted, vm[W_UP][:, columns], preferred_element_type=F32)
 
-    u_copies = {}
-    for j in far_first:
+    u_copies, r_copies = {}, {}
+
+    def for_partner(j):
         for q in range(1, tp):
             u_send[q - 1, j] = raised(j, q)
             u_copies[j, q] = send(
@@ -461,8 +482,8 @@
                 u_rs.at[q - 1, j],
                 {"tp": tp_peer(q)},
             )
-    r_copies = {}
-    for j in far_first:
+
+    def for_chip(j):
         total = raised(j, 0)
         for q in range(1, tp):
             u_copies[j, q].wait_recv()
@@ -474,6 +495,16 @@
             )
         else:
             own_sum[...] = total
+
+    for_partner(far_first[0])
+    for earlier, j in zip(far_first, far_first[1:]):
+        if j:
+            for_partner(j)
+            for_chip(earlier)
+        else:
+            for_chip(earlier)
+            for_partner(j)
+    for_chip(0)
     pending += list(u_copies.values()) + list(r_copies.values()) + q_copies
     sq_row = q_buf[0]
     for slot, copy in enumerate(q_copies, 1):
@@ -557,7 +588,7 @@
         for width in [named[name].shape[1] for name in (W_GATE, W_INPUT, W_BPROJ, W_CPROJ)]
         + [named[W_STEP].shape[0]]
     ]
-    wide = sum(pads) + LANES
+    wide, narrow = sum(pads[:-1]), pads[-1] + LANES
     channels = named[W_GATE].shape[1]
     share = named[W_OUT].shape[1] // tp
     all_rows = rows * dp
@@ -566,10 +597,10 @@
     row_lanes = -(-all_rows // LANES) * LANES
     dma = pltpu.SemaphoreType.DMA
     scratch = [pltpu.VMEM(named[name].shape, named[name].dtype) for name in COPIED] + [
-        pltpu.VMEM((kv, seqs, wide), F32),
-        pltpu.VMEM((kv - 1, seqs, wide), F32),
-        pltpu.VMEM((kv, seqs, channels + LANES), F32),
-        pltpu.VMEM((tp, rows, share + LANES), F32),
+        pltpu.VMEM((kv, seqs, wide), BF16),
+        pltpu.VMEM((kv - 1, seqs, wide), BF16),
+        pltpu.VMEM((kv, seqs, channels), BF16),
+        pltpu.VMEM((tp - 1, rows, share + LANES), F32),
         pltpu.VMEM((tp - 1, rows, share + LANES), F32),
         pltpu.VMEM((dp, rows, share), F32),
         pltpu.VMEM((kv * tp, 1, row_lanes), F32),
@@ -581,6 +612,9 @@
         pltpu.VMEM((kv * tp, all_rows, unit_share), BF16),
         pltpu.VMEM((dp, rows, columns), F32),
         pltpu.VMEM((dp - 1, rows, columns), F32),
+        pltpu.VMEM((kv, seqs, narrow), F32),
+        pltpu.VMEM((kv - 1, seqs, narrow), F32),
+        pltpu.VMEM((kv, seqs, LANES), F32),
         dma((len(COPIED),)),
         dma((kv - 1,)), dma((kv - 1,)),
         dma((kv - 1,)), dma((kv - 1,)),
@@ -592,6 +626,8 @@
         dma((kv - 1,)), dma((kv - 1,)),
         dma((tp - 1, kv)), dma((tp - 1, kv)),
         dma((dp - 1,)), dma((dp - 1,)),
+        dma((kv - 1,)), dma((kv - 1,)),
+        dma((kv - 1,)), dma((kv - 1,)),
     ]
     spaces = [
         pl.BlockSpec(memory_space=pltpu.SMEM if name == LENGTHS else pl.ANY) for name in NAMES

time: 35.6 us -> 35.7 us (level)
  no operation moved by 1% of the time
where the time goes in v3:
time: 35.7 us; the launch traced here: 35.4 us
  Pallas kernels  34.1 us (96%)
  local copies, waits for them, and re-layouts  1.3 us (4%)
    pallas_call x1, Pallas kernels, fused_device(): pl.pallas_call(functools.partial(fused, sizes), out_shape=jax.ShapeDtypeS...  34.1 us
    unnamed x1, local copies, waits for them, and re-layouts  1.3 us

profile of v3, /device:TPU:0, one launch (start us, length us, event | category | flops | bytes accessed | tf_op | source)
XLA Modules:
  0.0 35.4 jit_solution(13214972475646852935)
XLA Ops:
  0.0 34.1 %shard_map.235 = bf16[8,512]{1,0:T(8,128)(2,1)} custom-call(bf16[8,1024]{1,0:T(8,128)(2,1)} %refs_0_.1, f32[1,1024]{1,0:T(1,128)} %bitcast.15, bf16[1024,1024]{1,0:T(8,128)(2,1)} %refs_2_.1, bf16[1024,1024]{1,0:T(8,128)(2,1)} %refs_3_.1, bf16[1024,512]{1,0:T(8,128)(2,1)} %refs_4_.1, bf16[1024,512]{1,0:T(8,128)(2,1)} %refs_5_.1, bf16[16,1024]{1,0:T(8,128)(2,1)} %bitcast.10, ...), custom_call_target="tpu_custom_call" | custom-call | tf_op jit(solution)/shard_map/pallas_call | solution.py:635
  34.1 1.3 %copy.27 = bf16[8,512]{1,0:T(8,128)(2,1)} copy(bf16[8,512]{1,0:T(8,128)(2,1)} %shard_map.235) | data formatting | bytes 16384

commit v4 on v3

--- a/solution.py
+++ b/solution.py
@@ -465,16 +465,26 @@
     ]
     unit_share = vm[W_UP].shape[1] // (kv * tp)
 
-    def raised(j, q):
-        chunk = kv_peer(j) * tp + tp_peer(q)
-        columns = pl.ds(pl.multiple_of(chunk * unit_share, LANES), unit_share)
-        return jnp.dot(lifted, vm[W_UP][:, columns], preferred_element_type=F32)
+    def raised(j):
+        chip = kv_peer(j) * tp * unit_share
+        columns = pl.ds(pl.multiple_of(chip, LANES), tp * unit_share)
+        both = jnp.dot(lifted, vm[W_UP][:, columns], preferred_element_type=F32)
+        parts = [both[:, r * unit_share : (r + 1) * unit_share] for r in range(tp)]
+        picked = []
+        for q in range(tp):
+            piece = parts[0]
+            for r in range(1, tp):
+                piece = jnp.where(tp_peer(q) == r, parts[r], piece)
+            picked.append(piece)
+        return picked
 
     u_copies, r_copies = {}, {}
 
     def for_partner(j):
+        pieces = raised(j)
+        own_sum[j] = pieces[0]
         for q in range(1, tp):
-            u_send[q - 1, j] = raised(j, q)
+            u_send[q - 1, j] = pieces[q]
             u_copies[j, q] = send(
                 u_send.at[q - 1, j],
                 u_recv.at[q - 1, j],
@@ -484,7 +494,7 @@
             )
 
     def for_chip(j):
-        total = raised(j, 0)
+        total = own_sum[j]
         for q in range(1, tp):
             u_copies[j, q].wait_recv()
             total = total + u_recv[q - 1, j]
@@ -494,16 +504,12 @@
                 r_send.at[j - 1], r_recv.at[j - 1], r_ss.at[j - 1], r_rs.at[j - 1], {"kv": kv_peer(j)}
             )
         else:
-            own_sum[...] = total
+            own_sum[0] = total
 
     for_partner(far_first[0])
     for earlier, j in zip(far_first, far_first[1:]):
-        if j:
-            for_partner(j)
-            for_chip(earlier)
-        else:
-            for_chip(earlier)
-            for_partner(j)
+        for_partner(j)
+        for_chip(earlier)
     for_chip(0)
     pending += list(u_copies.values()) + list(r_copies.values()) + q_copies
     sq_row = q_buf[0]
@@ -512,7 +518,7 @@
         sq_row = sq_row + q_buf[slot]
     sq_sum = jnp.sum(jnp.where(row_eye, sq_row, 0.0), axis=1, keepdims=True)
     inverse_mlp = lax.rsqrt(sq_sum / features + EPS)
-    shares = own_sum[...]
+    shares = own_sum[0]
     for j in near_first:
         r_copies[j].wait_recv()
         shares = shares + r_recv[j - 1].astype(F32)
@@ -608,7 +614,7 @@
         pltpu.VMEM((tp - 1, kv, all_rows, unit_share), F32),
         pltpu.VMEM((kv - 1, all_rows, unit_share), BF16),
         pltpu.VMEM((kv - 1, all_rows, unit_share), BF16),
-        pltpu.VMEM((all_rows, unit_share), F32),
+        pltpu.VMEM((kv, all_rows, unit_share), F32),
         pltpu.VMEM((kv * tp, all_rows, unit_share), BF16),
         pltpu.VMEM((dp, rows, columns), F32),
         pltpu.VMEM((dp - 1, rows, columns), F32),

time: 35.7 us -> 35.4 us (level)
  no operation moved by 1% of the time
where the time goes in v4:
time: 35.4 us; the launch traced here: 35.1 us
  Pallas kernels  33.8 us (95%)
  local copies, waits for them, and re-layouts  1.3 us (4%)
    pallas_call x1, Pallas kernels, fused_device(): pl.pallas_call(functools.partial(fused, sizes), out_shape=jax.ShapeDtypeS...  33.8 us
    unnamed x1, local copies, waits for them, and re-layouts  1.3 us

profile of v4, /device:TPU:0, one launch (start us, length us, event | category | flops | bytes accessed | tf_op | source)
XLA Modules:
  0.0 35.1 jit_solution(13913508282321928261)
XLA Ops:
  0.0 33.8 %shard_map.235 = bf16[8,512]{1,0:T(8,128)(2,1)} custom-call(bf16[8,1024]{1,0:T(8,128)(2,1)} %refs_0_.1, f32[1,1024]{1,0:T(1,128)} %bitcast.15, bf16[1024,1024]{1,0:T(8,128)(2,1)} %refs_2_.1, bf16[1024,1024]{1,0:T(8,128)(2,1)} %refs_3_.1, bf16[1024,512]{1,0:T(8,128)(2,1)} %refs_4_.1, bf16[1024,512]{1,0:T(8,128)(2,1)} %refs_5_.1, bf16[16,1024]{1,0:T(8,128)(2,1)} %bitcast.10, ...), custom_call_target="tpu_custom_call" | custom-call | tf_op jit(solution)/shard_map/pallas_call | solution.py:641
  33.8 1.3 %copy.27 = bf16[8,512]{1,0:T(8,128)(2,1)} copy(bf16[8,512]{1,0:T(8,128)(2,1)} %shard_map.235) | data formatting | bytes 16384

commit v5 on v4

--- a/solution.py
+++ b/solution.py
@@ -175,7 +175,7 @@
 )
 MIDDLE = (
     CONV_INPUT, CONV_BPROJ, CONV_CPROJ, TAIL_INPUT, TAIL_BPROJ, TAIL_CPROJ,
-    STEP_BIAS, DECAY_LOG, BLOCK_STEP, BLOCK_BPROJ, BLOCK_INPUT, STATE,
+    LENGTHS, STEP_BIAS, DECAY_LOG, BLOCK_STEP, BLOCK_BPROJ, BLOCK_INPUT, STATE,
     GAIN_MIX, W_OUT, GAIN_MLP,
 )
 LATE = (W_UP, W_DOWN)
@@ -314,7 +314,7 @@
     decay_rate = column(-jnp.exp(vm[DECAY_LOG][...]))
     prepared = []
     for b in range(seqs):
-        live = positions < hbm[LENGTHS][b]
+        live = positions < vm[LENGTHS][b]
         steps = vm[BLOCK_STEP][b]
         masked = jnp.where(live, steps, 0.0)
         later = jnp.dot(
@@ -602,7 +602,10 @@
     columns = named[W_DOWN].shape[1]
     row_lanes = -(-all_rows // LANES) * LANES
     dma = pltpu.SemaphoreType.DMA
-    scratch = [pltpu.VMEM(named[name].shape, named[name].dtype) for name in COPIED] + [
+    scratch = [
+        (pltpu.SMEM if name == LENGTHS else pltpu.VMEM)(named[name].shape, named[name].dtype)
+        for name in COPIED
+    ] + [
         pltpu.VMEM((kv, seqs, wide), BF16),
         pltpu.VMEM((kv - 1, seqs, wide), BF16),
         pltpu.VMEM((kv, seqs, channels), BF16),
@@ -635,9 +638,7 @@
         dma((kv - 1,)), dma((kv - 1,)),
         dma((kv - 1,)), dma((kv - 1,)),
     ]
-    spaces = [
-        pl.BlockSpec(memory_space=pltpu.SMEM if name == LENGTHS else pl.ANY) for name in NAMES
-    ]
+    spaces = [pl.BlockSpec(memory_space=pl.ANY) for name in NAMES]
     return pl.pallas_call(
         functools.partial(fused, sizes),
         out_shape=jax.ShapeDtypeStruct((rows, columns), BF16),

time: 35.4 us -> 34.6 us (0.977)
  Pallas kernels: 33.8 us -> 33 us
    pallas_call x1, Pallas kernels: 33.8 us -> 33 us  [fused_device(): pl.pallas_call(functools.partial(fused, sizes), out_shape=jax.ShapeDtypeS...]
where the time goes in v5:
time: 34.6 us; the launch traced here: 34.3 us
  Pallas kernels  33 us (95%)
  local copies, waits for them, and re-layouts  1.3 us (4%)
    pallas_call x1, Pallas kernels, fused_device(): pl.pallas_call(functools.partial(fused, sizes), out_shape=jax.ShapeDtypeS...  33 us
    unnamed x1, local copies, waits for them, and re-layouts  1.3 us

profile of v5, /device:TPU:0, one launch (start us, length us, event | category | flops | bytes accessed | tf_op | source)
XLA Modules:
  0.0 34.3 jit_solution(13728306957255069566)
XLA Ops:
  0.0 33.0 %shard_map.235 = bf16[8,512]{1,0:T(8,128)(2,1)} custom-call(bf16[8,1024]{1,0:T(8,128)(2,1)} %refs_0_.1, f32[1,1024]{1,0:T(1,128)} %bitcast.15, bf16[1024,1024]{1,0:T(8,128)(2,1)} %refs_2_.1, bf16[1024,1024]{1,0:T(8,128)(2,1)} %refs_3_.1, bf16[1024,512]{1,0:T(8,128)(2,1)} %refs_4_.1, bf16[1024,512]{1,0:T(8,128)(2,1)} %refs_5_.1, bf16[16,1024]{1,0:T(8,128)(2,1)} %bitcast.10, ...), custom_call_target="tpu_custom_call" | custom-call | tf_op jit(solution)/shard_map/pallas_call | solution.py:642
  33.0 1.3 %copy.27 = bf16[8,512]{1,0:T(8,128)(2,1)} copy(bf16[8,512]{1,0:T(8,128)(2,1)} %shard_map.235) | data formatting | bytes 16384
